TPU v7x, 32 devices: a whole 2x2x4 slice. The times are simulated.
32 devices in a mesh: row: 8 (over z, core), col: 4 (over y, x).
Axes of the slice: x: 2, y: 2, z: 4, core: 2. Of those that a mesh axis runs over, the one named last changes fastest.
Arguments:
- tokens: bfloat16 [4096, 4096], P('row', 'col'), may hold values from -6 to 6
- norm_gain: float32 [4096], replicated, may hold values from 0.1 to 1.9
- out_weight: bfloat16 [4096, 4096], P(None, 'col'), may hold values from -0.09375 to 0.09375
Outputs:
- mixed: bfloat16 [4096, 4096], P('row', 'col')
All inputs are finite; a program needn't handle non-finite values.
Results may differ from a plain program's by a relative error of at most 0.015.
Values may be sent and summed in bfloat16 or wider, within the bound.
A program may use at most 64 MiB of HBM per device.

v0:
```python
import math
import numpy as np
import jax
import jax.numpy as jnp
from jax import lax
from jax.sharding import PartitionSpec as P

GROUPS = 4
EPSILON = 1e-06
PRECISE = lax.Precision.HIGHEST


def phases(left_idx, right_idx, period):
    product = left_idx[:, None] * right_idx[None, :] % period
    angles = product.astype(jnp.float32) * (2.0 * math.pi / period)
    return (jnp.cos(angles), jnp.sin(angles))


def split_table(table):
    table_high = table.astype(jnp.bfloat16)
    remainder = table - table_high.astype(jnp.float32)
    table_middle = remainder.astype(jnp.bfloat16)
    table_low = (remainder - table_middle.astype(jnp.float32)).astype(jnp.bfloat16)
    return (table_high, table_middle, table_low)


def host_tables(group_len, row_count, block_len):
    seq_len = block_len * row_count
    half = group_len // 2 // row_count
    slot = np.arange(group_len)
    freq = slot // (2 * half) * half + slot % half
    odd = slot // half % 2 == 1
    nyquist = odd & (freq == 0)
    sine = odd & ~nyquist
    freq = np.where(nyquist, group_len // 2, freq)
    chan = np.arange(group_len)
    angle = 2 * np.pi * (chan[:, None] * freq[None, :] % group_len) / group_len
    chan_table = np.where(sine[None, :], np.sin(angle), np.cos(angle)) / np.sqrt(group_len)
    low = np.arange(block_len)
    angle = 2 * np.pi * (low[:, None] * low[None, :] % block_len) / block_len
    low_table = np.concatenate([np.cos(angle), np.sin(angle)], 1) / np.sqrt(seq_len)
    high = np.arange(row_count)
    angle = 2 * np.pi * (high[:, None] * low[None, :] % seq_len) / seq_len
    return (chan_table, low_table, np.cos(angle), np.sin(angle))


def slot_facts(slot, group_len, row_count):
    half = group_len // 2 // row_count
    freq = slot // (2 * half) * half + slot % half
    odd = slot // half % 2 == 1
    nyquist = odd & (freq == 0)
    return (jnp.where(nyquist, group_len // 2, freq), odd & ~nyquist)


def folding(group_len, row_count):
    freq, sine = slot_facts(jnp.arange(group_len, dtype=jnp.int32), group_len, row_count)
    chan = jnp.arange(group_len, dtype=jnp.int32)[None, :]
    direct = chan == freq[:, None]
    mirror = chan == ((group_len - freq) % group_len)[:, None]
    signed = jnp.where(sine[:, None], -1.0, 1.0)
    return jnp.where(direct, signed, jnp.where(mirror, 1.0, 0.0)).astype(jnp.bfloat16)


def on_device_folded(tokens, norm_gain, out_weight):
    row_count = lax.axis_size("row")
    col_count = lax.axis_size("col")
    block_len, group_len = tokens.shape
    full_width = group_len * col_count
    slab = group_len // row_count
    out_width = out_weight.shape[1]
    chan_table, low_table, twist_cos, twist_sin = host_tables(group_len, row_count, block_len)
    chan_table = jnp.asarray(chan_table, jnp.bfloat16)
    low_table = jnp.asarray(low_table, jnp.bfloat16)
    twist_cos = jnp.asarray(twist_cos, jnp.float32)[:, :, None]
    twist_sin = jnp.asarray(twist_sin, jnp.float32)[:, :, None]
    values = tokens.astype(jnp.float32)
    total = lax.psum(jnp.sum(values * values, axis=-1), "col")
    inv_rms = lax.rsqrt(total / full_width + EPSILON)[:, None]
    gain = lax.dynamic_slice_in_dim(norm_gain, lax.axis_index("col") * group_len, group_len)
    normed = (values * inv_rms * gain).astype(jnp.bfloat16)
    chans = jnp.dot(normed, chan_table, preferred_element_type=jnp.float32).astype(jnp.bfloat16)
    moved = lax.all_to_all(chans, "row", split_axis=1, concat_axis=0, tiled=True)
    blocks = moved.reshape(row_count, block_len, slab).astype(jnp.float32)
    _, sine = slot_facts(
        lax.axis_index("row") * slab + jnp.arange(slab, dtype=jnp.int32), group_len, row_count
    )
    tops, bottoms = ([], [])
    for q in range(row_count):
        real, imag = (0.0, 0.0)
        for a in range(row_count):
            angle = 2 * math.pi * (a * q % row_count) / row_count
            real = real + blocks[a] * round(math.cos(angle), 12)
            imag = imag - blocks[a] * round(math.sin(angle), 12)
        turned_real = real * twist_cos[q] + imag * twist_sin[q]
        turned_imag = imag * twist_cos[q] - real * twist_sin[q]
        tops.append(jnp.where(sine, -turned_imag, turned_real).astype(jnp.bfloat16))
        bottoms.append(jnp.where(sine, turned_real, turned_imag).astype(jnp.bfloat16))
    stacked = jnp.concatenate([jnp.concatenate(tops, 1), jnp.concatenate(bottoms, 1)], 0)
    lows = jnp.dot(low_table, stacked, preferred_element_type=jnp.float32).astype(jnp.bfloat16)
    back = lax.all_to_all(
        lows.reshape(row_count, block_len // row_count, row_count * slab),
        "row",
        split_axis=0,
        concat_axis=0,
        tiled=True,
    )
    gathered = lax.all_gather(back, "col", axis=0, tiled=False)
    fold = folding(group_len, row_count)
    folded = jnp.einsum(
        "sm,gme->gse",
        fold,
        out_weight.reshape(col_count, group_len, out_width),
        preferred_element_type=jnp.float32,
    ).astype(jnp.bfloat16)
    mapped = jnp.einsum(
        "gspql,gsle->pqe",
        gathered.reshape(col_count, row_count, block_len // row_count, row_count, slab),
        folded.reshape(col_count, row_count, slab, out_width),
        preferred_element_type=jnp.float32,
    )
    return mapped.astype(jnp.bfloat16).reshape(block_len, out_width)


def on_device(tokens, norm_gain, out_weight):
    row_count = lax.axis_size("row")
    col_count = lax.axis_size("col")
    block_len, local_width = tokens.shape
    full_width = local_width * col_count
    group_len = full_width // GROUPS
    share_len = block_len // col_count
    seq_len = block_len * row_count
    slab_len = full_width // row_count
    col_index = lax.axis_index("col")
    chan_idx = jnp.arange(group_len, dtype=jnp.int32)
    cosines, sines = phases(chan_idx, chan_idx, group_len)
    chan_table = jnp.concatenate([cosines, sines], axis=1) / math.sqrt(group_len)
    table_parts = split_table(chan_table)
    arranged = tokens.reshape(col_count, share_len, local_width)
    portion = lax.all_to_all(arranged, "col", split_axis=0, concat_axis=2, tiled=True)
    item_count = portion.shape[1]
    values = portion.astype(jnp.float32)
    inv_rms = lax.rsqrt(jnp.mean(values * values, axis=-1, keepdims=True) + EPSILON)
    normed = lax.optimization_barrier((values * inv_rms * norm_gain).astype(jnp.bfloat16))
    grouped = normed.reshape(item_count, GROUPS, group_len)
    result = jnp.einsum("pgm,mj->pgj", grouped, table_parts[0], preferred_element_type=jnp.float32)
    result = result + jnp.einsum(
        "pgm,mj->pgj", grouped, table_parts[1], preferred_element_type=jnp.float32
    )
    result = result + jnp.einsum(
        "pgm,mj->pgj", grouped, table_parts[2], preferred_element_type=jnp.float32
    )
    high_idx = jnp.arange(row_count, dtype=jnp.int32)
    high_cos, high_sin = phases(high_idx, high_idx, row_count)
    high_table = jnp.concatenate(
        [jnp.concatenate([high_cos, -high_sin], 1), jnp.concatenate([-high_sin, -high_cos], 1)], 0
    )
    parts = (
        lax.all_to_all(
            result[..., :group_len].reshape(1, item_count, full_width),
            "row",
            split_axis=2,
            concat_axis=0,
            tiled=True,
        ),
        lax.all_to_all(
            result[..., group_len:].reshape(1, item_count, full_width),
            "row",
            split_axis=2,
            concat_axis=0,
            tiled=True,
        ),
    )
    item_count = parts[0].shape[1]
    stacked = jnp.concatenate(parts, 0).reshape(2 * row_count, item_count * slab_len)
    result = jnp.dot(high_table, stacked, precision=PRECISE)
    real_part = result[:row_count].reshape(row_count, item_count, slab_len)
    imag_part = result[row_count:].reshape(row_count, item_count, slab_len)
    local_pos = col_index * share_len + jnp.arange(share_len, dtype=jnp.int32)
    twist_cos, twist_sin = phases(high_idx, local_pos, seq_len)
    twist_cos = twist_cos[:, :, None]
    twist_sin = twist_sin[:, :, None]
    turned_real = real_part * twist_cos + imag_part * twist_sin
    turned_imag = imag_part * twist_cos - real_part * twist_sin
    low_idx = jnp.arange(block_len, dtype=jnp.int32)
    low_cos, low_sin = phases(low_idx, low_idx, block_len)
    low_cos = low_cos / math.sqrt(seq_len)
    low_sin = low_sin / math.sqrt(seq_len)
    low_table = jnp.concatenate([low_cos, low_sin], 1)
    stacked = jnp.concatenate(
        (
            lax.all_to_all(turned_real, "col", split_axis=0, concat_axis=1, tiled=True),
            lax.all_to_all(turned_imag, "col", split_axis=0, concat_axis=1, tiled=True),
        ),
        1,
    )
    finished = (jnp.einsum("ks,asc->akc", low_table, stacked, precision=PRECISE),)[0]
    spectrum = finished.astype(jnp.bfloat16)
    returned = lax.all_to_all(spectrum, "row", split_axis=1, concat_axis=2, tiled=True)
    mapped = jnp.einsum(
        "akd,de->kae",
        lax.all_gather(returned, "col", axis=0, tiled=True),
        out_weight,
        preferred_element_type=jnp.float32,
    )
    return mapped.astype(jnp.bfloat16).reshape(block_len, local_width)


def solution(mesh):

    def body(tokens, norm_gain, out_weight):
        whole_groups = tokens.shape[1] * GROUPS == out_weight.shape[0]
        program = on_device_folded if whole_groups else on_device
        return program(tokens, norm_gain, out_weight)

    placed = (P("row", "col"), P(), P(None, "col"))
    return jax.shard_map(
        body, mesh=mesh, in_specs=placed, out_specs=P("row", "col"), check_vma=False
    )
```

profile of v0, /device:TPU:0, one launch (start us, length us, event | category | flops | bytes accessed | tf_op | source)
XLA Modules:
  0.0 159.7 jit_solution(6261747024273125081)
XLA Ops:
  6.5 1.5 fusion
  8.0 11.4 %psum.7 = f32[512]{0:T(512)S(1)} all-reduce(f32[512]{0:T(512)S(1)} %fusion), channel_id=1, replica_groups=mesh['row'=8,'col'=4] {'col'}, use_global_device_ids=true, to_apply=%region_1.0 | all-reduce | flops 512 | bytes 4096 | tf_op jit(solution)/shard_map/psum | solution.py:77
  19.4 0.7 dynamic_slice.3
  20.1 3.2 %fusion.10 = bf16[64,8,8,128]{3,2,1,0:T(8,128)(2,1)S(1)} fusion(bf16[1024,1024]{1,0:T(8,128)(2,1)} %constant.151.clone, bf16[512,1024]{1,0:T(8,128)(2,1)} %param.7, f32[1024]{0:T(1024)S(1)} %dynamic_slice.3, f32[512]{0:T(512)S(1)} %add_rsqrt_fusion), kind=kOutput, calls=%fused_computation.19 | convolution fusion | flops 1076363264 | bytes 4200448 | tf_op jit(solution)/shard_map/dot_general | solution.py:81
  23.4 1.2 copy.26
  24.5 4.9 %all-to-all-start = ((bf16[512,8,128]{2,0,1:T(8,128)(2,1)}), bf16[512,8,128]{2,0,1:T(8,128)(2,1)S(1)}, u32[]{:S(2)}, u32[]{:S(2)}) async-start(bf16[512,8,128]{2,0,1:T(8,128)(2,1)} %bitcast.434), calls=%async_computation | async-start | bytes 2097152 | tf_op jit(solution)/shard_map/all_to_all | solution.py:82
  29.5 26.5 %all-to-all-done = bf16[512,8,128]{2,0,1:T(8,128)(2,1)S(1)} async-done(((bf16[512,8,128]{2,0,1:T(8,128)(2,1)}), bf16[512,8,128]{2,0,1:T(8,128)(2,1)S(1)}, u32[]{:S(2)}, u32[]{:S(2)}) %all-to-all-start) | async-done | bytes 1048608 | tf_op jit(solution)/shard_map/all_to_all | solution.py:82
  56.4 0.4 copy-done.14
  56.8 0.4 fusion.24
  57.2 0.4 fusion.25
  57.7 0.4 fusion.26
  58.1 0.3 fusion.27
  58.4 0.3 copy-done.4
  58.8 0.4 fusion.28
  59.2 0.4 fusion.29
  59.6 0.5 fusion.30
  61.7 0.7 fusion.50
  62.5 0.7 add_convert_fusion
  63.2 29.7 %all_to_all.18 = bf16[8,64,1024]{2,1,0:T(8,128)(2,1)} all-to-all(bf16[8,64,1024]{2,1,0:T(8,128)(2,1)S(1)} %bitcast.437), channel_id=1, replica_groups=mesh['row'=8,'col'=4] {'row'}, dimensions={0} | all-to-all | bytes 2097152 | tf_op jit(solution)/shard_map/all_to_all | solution.py:100
  93.0 14.8 %convolution_convert_fusion = bf16[1024,4,1024]{2,0,1:T(8,128)(2,1)} fusion(bf16[4,1024,1024]{2,1,0:T(8,128)(2,1)} %bitcast.438, s32[1024]{0:T(1024)S(1)} %get-tuple-element.30, bf16[1024]{0:T(1024)(128)(2,1)S(1)} %and_select_fusion, s32[1024]{0:T(1024)S(1)} %get-tuple-element.31), kind=kOutput, calls=%fused_computation | convolution fusion | flops 8598323200 | bytes 16787456 | tf_op jit(solution)/shard_map/sm,gme->gse/dot_general | solution.py:109
  107.7 35.0 %all-gather.3.cloned.1.call-done = bf16[32,64,1024]{2,1,0:T(8,128)(2,1)} async-done(((bf16[8,64,1024]{2,1,0:T(8,128)(2,1)}), bf16[32,64,1024]{2,1,0:T(8,128)(2,1)}) %all-gather.3.cloned.1.call-update) | async-done | bytes 4194320 | tf_op jit(solution)/shard_map/all_gather | solution.py:107
  142.7 3.5 %copy.24 = bf16[256,8,8,128]{3,2,1,0:T(8,128)(2,1)S(1)} copy(bf16[256,8,8,128]{3,1,2,0:T(8,128)(2,1)} %bitcast.435) | data formatting | bytes 8388608
  146.2 1.1 copy-done.16
  147.3 5.5 %fusion.11 = bf16[512,1024]{1,0:T(8,128)(2,1)} fusion(bf16[4,8,64,8,128]{4,3,2,1,0:T(8,128)(2,1)S(1)} %bitcast.436, bf16[4,8,128,1024,1]{3,2,4,1,0:T(8,128)(2,1)S(1)} %bitcast.439), kind=kOutput, calls=%fused_computation.20 | convolution fusion | flops 4295491584 | bytes 13631488 | tf_op jit(solution)/shard_map/gspql,gsle->pqe/dot_general | solution.py:115
  (45 shorter events, 2.2 us)
Async XLA Ops:
  24.5 31.4 %all-to-all-start = ((bf16[512,8,128]{2,0,1:T(8,128)(2,1)}), bf16[512,8,128]{2,0,1:T(8,128)(2,1)S(1)}, u32[]{:S(2)}, u32[]{:S(2)}) async-start(bf16[512,8,128]{2,0,1:T(8,128)(2,1)} %bitcast.434), calls=%async_computation | async-start | bytes 2097152 | tf_op jit(solution)/shard_map/all_to_all | solution.py:82
  29.4 113.3 %all-gather.3.cloned.1.call-start = ((), (), s32[]{:S(2)}) async-start(), calls=%async_computation.2 | async-start | bytes 5242880 | tf_op jit(solution)/shard_map/all_gather | solution.py:107
  56.1 0.7 copy-start.14
  56.1 0.7 copy-start.15
  56.1 1.1 copy-start.8
  56.1 1.1 copy-start.9
  56.8 0.8 copy-start.6
  56.8 0.8 copy-start.7
  57.2 0.9 copy-start.12
  57.2 0.9 copy-start.13
  58.1 0.7 copy-start.4
  58.1 0.7 copy-start.5
  58.4 0.8 copy-start.2
  58.4 0.8 copy-start.3
  58.8 0.8 copy-start.10
  58.8 0.8 copy-start.11
  60.1 1.6 %copy-start.1 = (bf16[512,512]{1,0:T(8,128)(2,1)S(1)}, bf16[512,512]{1,0:T(8,128)(2,1)}, u32[]{:S(2)}) copy-start(bf16[512,512]{1,0:T(8,128)(2,1)} %constant.187) | copy-start | bytes 1572868
  61.4 1.0 copy-start
  142.7 4.6 %copy-start.16 = (bf16[1024,4,1024]{2,0,1:T(8,128)(2,1)S(1)}, bf16[1024,4,1024]{2,0,1:T(8,128)(2,1)}, u32[]{:S(2)}) copy-start(bf16[1024,4,1024]{2,0,1:T(8,128)(2,1)} %convolution_convert_fusion) | copy-start | bytes 25165828
Sparse Core Ops, SparseCore 0:
  93.0 49.6 all-gather.2
where the time goes:
time: 160 us
  waiting for transfers between devices  61.5 us (38%)
  blocking collectives  41.1 us (26%)
  matrix products  24.9 us (16%)
  between operations  13.7 us (9%)
  local copies, waits for them, and re-layouts  7.33 us (5%)
  other arithmetic  6.34 us (4%)
  starting transfers between devices  4.91 us (3%)
    all_gather x1, waiting for transfers between devices, on_device_folded(): gathered = lax.all_gather(back, 'col', axis=0, tiled=False)  35 us
    all_to_all x1, blocking collectives, on_device_folded(): lax.all_to_all(lows.reshape(row_count, block_len // row_count, row_count...  29.7 us
    all_to_all x1, waiting for transfers between devices, on_device_folded(): lax.all_to_all(chans, 'row', split_axis=1, concat_axis=0, tiled=True)  26.5 us
    dot_general x1, matrix products, on_device_folded(): jnp.einsum('sm,gme->gse', fold, out_weight.reshape(col_count, group_len,...  14.8 us
    psum x1, blocking collectives, on_device_folded(): total = lax.psum(jnp.sum(values * values, axis=-1), 'col')  11.4 us
    dot_general x1, matrix products, on_device_folded(): jnp.einsum('gspql,gsle->pqe', gathered.reshape(col_count, row_count, bloc...  5.52 us
    unnamed x35, local copies, waits for them, and re-layouts  5.47 us
    all_to_all x1, starting transfers between devices, on_device_folded(): lax.all_to_all(chans, 'row', split_axis=1, concat_axis=0, tiled=True)  4.87 us
  transfers between devices with their start and end apart: 2, of which 2 were waited for; matrix products, arithmetic and copies ran while one was open for 9% of the time, Pallas kernels for 0%

commit v1 on v0

--- a/solution.py
+++ b/solution.py
@@ -4,6 +4,7 @@
 import jax.numpy as jnp
 from jax import lax
 from jax.sharding import PartitionSpec as P
+from jax.lax import all_gather
 
 GROUPS = 4
 EPSILON = 1e-06
@@ -74,7 +75,7 @@
     twist_cos = jnp.asarray(twist_cos, jnp.float32)[:, :, None]
     twist_sin = jnp.asarray(twist_sin, jnp.float32)[:, :, None]
     values = tokens.astype(jnp.float32)
-    total = lax.psum(jnp.sum(values * values, axis=-1), "col")
+    total = jnp.sum(all_gather(jnp.sum(values * values, axis=-1), "col"), axis=0)
     inv_rms = lax.rsqrt(total / full_width + EPSILON)[:, None]
     gain = lax.dynamic_slice_in_dim(norm_gain, lax.axis_index("col") * group_len, group_len)
     normed = (values * inv_rms * gain).astype(jnp.bfloat16)

time: 160 us -> 159 us (level)
  blocking collectives: 41.1 us -> 39.3 us
    psum x1 -> x0, blocking collectives: 11.4 us -> none  [on_device_folded(): total = lax.psum(jnp.sum(values * values, axis=-1), 'col')]
    all_gather x0 -> x1, blocking collectives: none -> 9.57 us  [on_device_folded(): all_gather(jnp.sum(values * values, axis=-1), 'col')]
where the time goes in v1:
time: 159 us
  waiting for transfers between devices  62.4 us (39%)
  blocking collectives  39.3 us (25%)
  matrix products  24.9 us (16%)
  between operations  13.7 us (9%)
  local copies, waits for them, and re-layouts  7.33 us (5%)
  other arithmetic  6.36 us (4%)
  starting transfers between devices  4.93 us (3%)
    all_gather x1, waiting for transfers between devices, on_device_folded(): gathered = lax.all_gather(back, 'col', axis=0, tiled=False)  35.9 us
    all_to_all x1, blocking collectives, on_device_folded(): lax.all_to_all(lows.reshape(row_count, block_len // row_count, row_count...  29.7 us
    all_to_all x1, waiting for transfers between devices, on_device_folded(): lax.all_to_all(chans, 'row', split_axis=1, concat_axis=0, tiled=True)  26.5 us
    dot_general x1, matrix products, on_device_folded(): jnp.einsum('sm,gme->gse', fold, out_weight.reshape(col_count, group_len,...  14.8 us
    all_gather x1, blocking collectives, on_device_folded(): all_gather(jnp.sum(values * values, axis=-1), 'col')  9.57 us
    dot_general x1, matrix products, on_device_folded(): jnp.einsum('gspql,gsle->pqe', gathered.reshape(col_count, row_count, bloc...  5.52 us
    unnamed x35, local copies, waits for them, and re-layouts  5.47 us
    all_to_all x1, starting transfers between devices, on_device_folded(): lax.all_to_all(chans, 'row', split_axis=1, concat_axis=0, tiled=True)  4.89 us
  transfers between devices with their start and end apart: 2, of which 2 were waited for; matrix products, arithmetic and copies ran while one was open for 9% of the time, Pallas kernels for 0%

profile of v1, /device:TPU:0, one launch (start us, length us, event | category | flops | bytes accessed | tf_op | source)
XLA Modules:
  0.0 158.9 jit_solution(18290271655385250812)
XLA Ops:
  6.5 1.5 fusion
  8.0 9.6 %all-gather.2 = f32[4,1,512]{2,1,0:T(1,128)S(1)} all-gather(f32[1,1,512]{2,1,0:T(1,128)S(1)} %bitcast.439), channel_id=2, replica_groups=mesh['row'=8,'col'=4] {'col'}, dimensions={0}, use_global_device_ids=true | all-gather | bytes 10240 | tf_op jit(solution)/shard_map/all_gather | solution.py:78
  17.6 0.7 dynamic_slice.3
  18.3 3.2 %fusion.10 = bf16[64,8,8,128]{3,2,1,0:T(8,128)(2,1)S(1)} fusion(bf16[1024,1024]{1,0:T(8,128)(2,1)} %constant.151.clone, bf16[512,1024]{1,0:T(8,128)(2,1)} %param.7, f32[1024]{0:T(1024)S(1)} %dynamic_slice.3, f32[512]{0:T(512)S(1)} %add_rsqrt_fusion), kind=kOutput, calls=%fused_computation.19 | convolution fusion | flops 1076363264 | bytes 4200448 | tf_op jit(solution)/shard_map/dot_general | solution.py:82
  21.6 1.2 copy.26
  22.7 4.9 %all-to-all-start = ((bf16[512,8,128]{2,0,1:T(8,128)(2,1)}), bf16[512,8,128]{2,0,1:T(8,128)(2,1)S(1)}, u32[]{:S(2)}, u32[]{:S(2)}) async-start(bf16[512,8,128]{2,0,1:T(8,128)(2,1)} %bitcast.435), calls=%async_computation | async-start | bytes 2097152 | tf_op jit(solution)/shard_map/all_to_all | solution.py:83
  27.7 26.5 %all-to-all-done = bf16[512,8,128]{2,0,1:T(8,128)(2,1)S(1)} async-done(((bf16[512,8,128]{2,0,1:T(8,128)(2,1)}), bf16[512,8,128]{2,0,1:T(8,128)(2,1)S(1)}, u32[]{:S(2)}, u32[]{:S(2)}) %all-to-all-start) | async-done | bytes 1048608 | tf_op jit(solution)/shard_map/all_to_all | solution.py:83
  54.6 0.4 copy-done.14
  55.0 0.4 fusion.24
  55.5 0.4 fusion.25
  55.9 0.4 fusion.26
  56.3 0.3 fusion.27
  56.6 0.3 copy-done.4
  57.0 0.4 fusion.28
  57.4 0.4 fusion.29
  57.8 0.5 fusion.30
  60.0 0.7 fusion.50
  60.7 0.7 add_convert_fusion
  61.4 29.7 %all_to_all.18 = bf16[8,64,1024]{2,1,0:T(8,128)(2,1)} all-to-all(bf16[8,64,1024]{2,1,0:T(8,128)(2,1)S(1)} %bitcast.438), channel_id=1, replica_groups=mesh['row'=8,'col'=4] {'row'}, dimensions={0} | all-to-all | bytes 2097152 | tf_op jit(solution)/shard_map/all_to_all | solution.py:101
  91.2 14.8 %convolution_convert_fusion = bf16[1024,4,1024]{2,0,1:T(8,128)(2,1)} fusion(bf16[4,1024,1024]{2,1,0:T(8,128)(2,1)} %bitcast.440, s32[1024]{0:T(1024)S(1)} %get-tuple-element.30, bf16[1024]{0:T(1024)(128)(2,1)S(1)} %and_select_fusion, s32[1024]{0:T(1024)S(1)} %get-tuple-element.31), kind=kOutput, calls=%fused_computation | convolution fusion | flops 8598323200 | bytes 16787456 | tf_op jit(solution)/shard_map/sm,gme->gse/dot_general | solution.py:110
  106.0 35.9 %all-gather.5.cloned.1.call-done = bf16[32,64,1024]{2,1,0:T(8,128)(2,1)} async-done(((bf16[8,64,1024]{2,1,0:T(8,128)(2,1)}), bf16[32,64,1024]{2,1,0:T(8,128)(2,1)}) %all-gather.5.cloned.1.call-update) | async-done | bytes 4194320 | tf_op jit(solution)/shard_map/all_gather | solution.py:108
  141.8 3.5 %copy.24 = bf16[256,8,8,128]{3,2,1,0:T(8,128)(2,1)S(1)} copy(bf16[256,8,8,128]{3,1,2,0:T(8,128)(2,1)} %bitcast.436) | data formatting | bytes 8388608
  145.3 1.1 copy-done.16
  146.5 5.5 %fusion.11 = bf16[512,1024]{1,0:T(8,128)(2,1)} fusion(bf16[4,8,64,8,128]{4,3,2,1,0:T(8,128)(2,1)S(1)} %bitcast.437, bf16[4,8,128,1024,1]{3,2,4,1,0:T(8,128)(2,1)S(1)} %bitcast.441), kind=kOutput, calls=%fused_computation.20 | convolution fusion | flops 4295491584 | bytes 13631488 | tf_op jit(solution)/shard_map/gspql,gsle->pqe/dot_general | solution.py:116
  (46 shorter events, 2.3 us)
Async XLA Ops:
  22.7 31.5 %all-to-all-start = ((bf16[512,8,128]{2,0,1:T(8,128)(2,1)}), bf16[512,8,128]{2,0,1:T(8,128)(2,1)S(1)}, u32[]{:S(2)}, u32[]{:S(2)}) async-start(bf16[512,8,128]{2,0,1:T(8,128)(2,1)} %bitcast.435), calls=%async_computation | async-start | bytes 2097152 | tf_op jit(solution)/shard_map/all_to_all | solution.py:83
  27.6 114.2 %all-gather.5.cloned.1.call-start = ((), (), s32[]{:S(2)}) async-start(), calls=%async_computation.2 | async-start | bytes 5242880 | tf_op jit(solution)/shard_map/all_gather | solution.py:108
  54.3 0.7 copy-start.14
  54.3 0.7 copy-start.15
  54.3 1.1 copy-start.8
  54.4 1.1 copy-start.9
  55.0 0.8 copy-start.6
  55.0 0.8 copy-start.7
  55.4 0.9 copy-start.12
  55.5 0.9 copy-start.13
  56.3 0.7 copy-start.4
  56.3 0.7 copy-start.5
  56.6 0.8 copy-start.2
  56.6 0.8 copy-start.3
  57.0 0.8 copy-start.10
  57.0 0.8 copy-start.11
  58.3 1.6 %copy-start.1 = (bf16[512,512]{1,0:T(8,128)(2,1)S(1)}, bf16[512,512]{1,0:T(8,128)(2,1)}, u32[]{:S(2)}) copy-start(bf16[512,512]{1,0:T(8,128)(2,1)} %constant.187) | copy-start | bytes 1572868
  59.7 1.0 copy-start
  141.8 4.6 %copy-start.16 = (bf16[1024,4,1024]{2,0,1:T(8,128)(2,1)S(1)}, bf16[1024,4,1024]{2,0,1:T(8,128)(2,1)}, u32[]{:S(2)}) copy-start(bf16[1024,4,1024]{2,0,1:T(8,128)(2,1)} %convolution_convert_fusion) | copy-start | bytes 25165828
Sparse Core Ops, SparseCore 0:
  91.3 50.5 all-gather.4
